TPU v7x, 32 devices: a whole 2x2x4 slice. The times are simulated.
32 devices in a mesh: sp: 8 (over z, y), tp: 4 (over x, core).
Axes of the slice: x: 2, y: 2, z: 4, core: 2. Of those that a mesh axis runs over, the one named last changes fastest.
Arguments:
- tokens: bfloat16 [2048, 2048], P(('sp', 'tp')), may hold values from -6 to 6
- pre_gain: float32 [2048], replicated, may hold values from 0.1 to 1.9
- w_query_ret: bfloat16 [2048, 768], P('sp', 'tp'), may hold values from -0.125 to 0.125
- w_key_ret: bfloat16 [2048, 768], P('sp', 'tp'), may hold values from -0.125 to 0.125
- w_value_ret: bfloat16 [2048, 768], P('sp', 'tp'), may hold values from -0.125 to 0.125
- w_query_att: bfloat16 [2048, 768], P('sp', 'tp'), may hold values from -0.5 to 0.5
- w_key_att: bfloat16 [2048, 256], P('sp', 'tp'), may hold values from -0.125 to 0.125
- w_value_att: bfloat16 [2048, 256], P('sp', 'tp'), may hold values from -0.125 to 0.125
- w_out_ret: bfloat16 [768, 2048], P('tp', 'sp'), may hold values from -0.15625 to 0.15625
- w_out_att: bfloat16 [768, 2048], P('tp', 'sp'), may hold values from -0.15625 to 0.15625
- retain_log: float32 [2048, 12], P('sp', 'tp')
- forget_total: float32 [12, 2048], P('tp'), as said below
Outputs:
- mixed: bfloat16 [2048, 2048], P(('sp', 'tp'))
Inputs may be any that keep to these rules, and one draw needn't show every extreme that they name: `forget_total`: never rises along positions.
All inputs are finite; a program needn't handle non-finite values.
Results may differ from a plain program's by a relative error of at most 0.019.
Values may be sent and summed in bfloat16 or wider, within the bound.
A program may use at most 64 MiB of HBM per device.

v0:
```python
import jax
import jax.numpy as jnp
from jax import lax
from jax.sharding import PartitionSpec as P

HEAD = 64
SPAN = 256
KEY_SPAN = 256


EPS = 1e-06
THETA = 10000.0
HIGH = lax.Precision.HIGHEST


def rotate(field, positions):
    half = field.shape[-1] // 2
    inverse = THETA ** (-jnp.arange(half, dtype=jnp.float32) / half)
    angles = positions[:, None] * inverse[None, :]
    cosine = jnp.cos(angles)[:, None, :]
    sine = jnp.sin(angles)[:, None, :]
    first_half = field[..., :half]
    second_half = field[..., half:]
    return jnp.concatenate(
        [first_half * cosine - second_half * sine, first_half * sine + second_half * cosine],
        axis=-1,
    )


def head_norm(values):
    centre = jnp.mean(values, axis=-1, keepdims=True)
    spread = jnp.mean(jnp.square(values - centre), axis=-1, keepdims=True)
    return (values - centre) * lax.rsqrt(spread + EPS)


def advance(state, pair):
    decay, update = pair
    return (jnp.exp(decay)[:, None, None] * state + update, state)


def body(
    tokens,
    pre_gain,
    w_query_ret,
    w_key_ret,
    w_value_ret,
    w_query_att,
    w_key_att,
    w_value_att,
    w_out_ret,
    w_out_att,
    retain_log,
    forget_total,
):
    rows = tokens.astype(jnp.float32)
    normed = (
        rows * lax.rsqrt(jnp.mean(rows * rows, axis=-1, keepdims=True) + EPS) * pre_gain
    ).astype(jnp.bfloat16)
    gathered = lax.all_gather(normed, "tp", axis=0, tiled=True)
    tok_dev = gathered.shape[0]
    offset = lax.axis_index("sp") * tok_dev
    query_places = offset + jnp.arange(tok_dev, dtype=jnp.int32)
    positions = query_places.astype(jnp.float32)

    def blocked(values):
        return values.reshape((tok_dev // SPAN, SPAN) + values.shape[1:])

    pieces = (
        lax.all_gather(w_query_ret, "sp", axis=0, tiled=True),
        lax.all_gather(w_key_ret, "sp", axis=0, tiled=True),
        lax.all_gather(w_value_ret, "sp", axis=0, tiled=True),
        lax.all_gather(w_query_att, "sp", axis=0, tiled=True),
        lax.all_gather(w_key_att, "sp", axis=0, tiled=True),
        lax.all_gather(w_value_att, "sp", axis=0, tiled=True),
    )
    projected = tuple(
        (jnp.dot(gathered, piece, preferred_element_type=jnp.float32) for piece in pieces)
    )
    heads = retain_log.shape[1]
    shape = (tok_dev, heads, HEAD)
    query = blocked(
        (rotate(projected[0].reshape(shape), positions) * HEAD ** (-0.5)).astype(jnp.bfloat16)
    )
    key_rows = blocked(rotate(projected[1].reshape(shape), positions).astype(jnp.bfloat16))
    value_rows = blocked(projected[2].astype(jnp.bfloat16).reshape(shape))
    within = jnp.cumsum(blocked(retain_log), axis=1)
    causal = jnp.arange(SPAN)[:, None] >= jnp.arange(SPAN)[None, :]
    scores = jnp.einsum("bthd,bshd->bhts", query, key_rows, preferred_element_type=jnp.float32)
    turned = jnp.transpose(within, (0, 2, 1))
    gap = jnp.where(causal, turned[:, :, :, None] - turned[:, :, None, :], 0.0)
    weights = jnp.where(causal, scores * jnp.exp(gap), 0.0).astype(jnp.bfloat16)
    local = jnp.einsum("bhts,bshd->bthd", weights, value_rows, preferred_element_type=jnp.float32)
    last = within[:, -1]
    faded = (key_rows.astype(jnp.float32) * jnp.exp(last[:, None, :] - within)[..., None]).astype(
        jnp.bfloat16
    )
    updates = jnp.einsum("bshd,bshe->bhde", faded, value_rows, preferred_element_type=jnp.float32)
    zero_state = jnp.zeros((heads, HEAD, HEAD), jnp.float32)
    final, _ = lax.scan(advance, zero_state, (last, updates))
    decay_total = jnp.sum(last, axis=0)
    own_state = final.reshape(heads, HEAD * HEAD)
    every_total = lax.all_gather(
        decay_total[None].astype(jnp.bfloat16), "sp", axis=0, tiled=True
    ).astype(jnp.float32)
    every_state = lax.all_gather(
        own_state[None].astype(jnp.bfloat16), "sp", axis=0, tiled=True
    ).astype(jnp.float32)
    device_order = jnp.arange(every_total.shape[0], dtype=jnp.int32)[:, None]
    earlier = device_order < lax.axis_index("sp")
    before = jnp.sum(jnp.where(earlier, every_total, 0.0), axis=0)
    through = jnp.cumsum(every_total, axis=0)
    fading = jnp.where(earlier, jnp.exp(jnp.where(earlier, before[None, :] - through, 0.0)), 0.0)
    incoming = jnp.einsum("jh,jhe->he", fading, every_state, precision=HIGH)
    _, befores = lax.scan(advance, incoming.reshape(heads, HEAD, HEAD), (last, updates))
    lifted = (query.astype(jnp.float32) * jnp.exp(within)[..., None]).astype(jnp.bfloat16)
    carried = jnp.einsum(
        "bthd,bhde->bthe", lifted, befores.astype(jnp.bfloat16), preferred_element_type=jnp.float32
    )
    retained = (
        head_norm((local + carried).reshape(shape))
        .astype(jnp.bfloat16)
        .reshape(tok_dev, heads * HEAD)
    )
    raw_key = projected[4]
    gate_heads = forget_total.shape[0]
    kv_local = raw_key.shape[1] // HEAD
    group = gate_heads // kv_local
    query = (
        (projected[3] * HEAD ** (-0.5)).astype(jnp.bfloat16).reshape(tok_dev, kv_local, group, HEAD)
    )
    key_rows = raw_key.astype(jnp.bfloat16)
    value_rows = projected[5].astype(jnp.bfloat16)
    gate_rows = lax.dynamic_slice_in_dim(forget_total, offset, tok_dev, 1).reshape(
        kv_local, group, tok_dev
    )
    last_row = offset + tok_dev - 1
    init = (
        jnp.zeros((kv_local, group, tok_dev, HEAD), jnp.float32),
        jnp.zeros((kv_local, group, tok_dev), jnp.float32),
    )
    key_piece = lax.all_gather(key_rows, "sp", axis=0, tiled=True)
    value_piece = lax.all_gather(value_rows, "sp", axis=0, tiled=True)
    count = key_piece.shape[0] // KEY_SPAN

    def one_block(index, inner):
        first = index * KEY_SPAN

        def compute(state):
            weighted, total = state
            key_block = lax.dynamic_slice_in_dim(key_piece, index * KEY_SPAN, KEY_SPAN, 0).reshape(
                KEY_SPAN, kv_local, HEAD
            )
            value_block = lax.dynamic_slice_in_dim(
                value_piece, index * KEY_SPAN, KEY_SPAN, 0
            ).reshape(KEY_SPAN, kv_local, HEAD)
            gate_keys = lax.dynamic_slice_in_dim(forget_total, first, KEY_SPAN, 1).reshape(
                kv_local, group, KEY_SPAN
            )
            scores = jnp.einsum(
                "tcgd,scd->cgts", query, key_block, preferred_element_type=jnp.float32
            )
            logits = scores + gate_rows[:, :, :, None] - gate_keys[:, :, None, :]
            allowed = (first + jnp.arange(KEY_SPAN, dtype=jnp.int32))[None, :] <= query_places[
                :, None
            ]
            weights = jnp.exp(jnp.where(allowed, logits, -jnp.inf))
            total = total + jnp.sum(weights, axis=-1)
            weighted = weighted + jnp.einsum(
                "cgts,scd->cgtd",
                weights.astype(jnp.bfloat16),
                value_block,
                preferred_element_type=jnp.float32,
            )
            return (weighted, total)

        def skipped(state):
            return state

        return lax.cond(first <= last_row, compute, skipped, inner)

    weighted, total = lax.fori_loop(0, count, one_block, init)
    result = weighted / total[..., None]
    attended = (
        jnp.transpose(result, (2, 0, 1, 3)).reshape(tok_dev, gate_heads * HEAD).astype(jnp.bfloat16)
    )
    out_ret, out_att = (
        lax.all_gather(w_out_ret, "sp", axis=1, tiled=True),
        lax.all_gather(w_out_att, "sp", axis=1, tiled=True),
    )
    return lax.psum_scatter(
        (
            jnp.dot(retained, out_ret, preferred_element_type=jnp.float32)
            + jnp.dot(attended, out_att, preferred_element_type=jnp.float32)
        ).astype(jnp.bfloat16),
        "tp",
        scatter_dimension=0,
        tiled=True,
    )


def solution(mesh):
    return jax.shard_map(
        body,
        mesh=mesh,
        in_specs=(
            P(("sp", "tp"), None),
            P(),
            P("sp", "tp"),
            P("sp", "tp"),
            P("sp", "tp"),
            P("sp", "tp"),
            P("sp", "tp"),
            P("sp", "tp"),
            P("tp", "sp"),
            P("tp", "sp"),
            P("sp", "tp"),
            P("tp", None),
        ),
        out_specs=P(("sp", "tp"), None),
        check_vma=False,
    )
```

profile of v0, /device:TPU:1, one launch (start us, length us, event | category | flops | bytes accessed | tf_op | source)
XLA Modules:
  0.0 462.1 jit_solution(11235559087776837710)
XLA Ops:
  6.6 1.2 fusion.24
  7.8 1.8 fusion.26
  10.4 0.9 reduce-window.6
  11.7 18.0 %all-gather = bf16[8,1,3]{2,1,0:T(2,128)(2,1)S(1)} all-gather(bf16[1,1,3]{2,1,0:T(2,128)(2,1)S(1)} %slice.47), channel_id=2, replica_groups=mesh['sp'=8,'tp'=4] {'sp'}, dimensions={0}, use_global_device_ids=true | all-gather | bytes 54 | tf_op jit(solution)/shard_map/all_gather | solution.py:102
  31.0 26.9 %all_gather.46 = bf16[2048,64]{0,1:T(8,128)(2,1)} all-gather(bf16[256,64]{0,1:T(8,128)(2,1)S(1)} %copy-done.9), channel_id=1, replica_groups=mesh['sp'=8,'tp'=4] {'sp'}, dimensions={0}, use_global_device_ids=true | all-gather | bytes 294912 | tf_op jit(solution)/shard_map/all_gather | solution.py:73
  57.9 26.4 %all_gather.49 = bf16[2048,64]{0,1:T(8,128)(2,1)} all-gather(bf16[256,64]{0,1:T(8,128)(2,1)S(1)} %copy-done.10), channel_id=1, replica_groups=mesh['sp'=8,'tp'=4] {'sp'}, dimensions={0}, use_global_device_ids=true | all-gather | bytes 294912 | tf_op jit(solution)/shard_map/all_gather | solution.py:74
  84.2 27.6 %all_gather.41 = bf16[2048,192]{0,1:T(8,128)(2,1)} all-gather(bf16[256,192]{0,1:T(8,128)(2,1)S(1)} %copy-done.3), channel_id=1, replica_groups=mesh['sp'=8,'tp'=4] {'sp'}, dimensions={0}, use_global_device_ids=true | all-gather | bytes 884736 | tf_op jit(solution)/shard_map/all_gather | solution.py:69
  111.9 26.6 %all_gather.42 = bf16[2048,192]{0,1:T(8,128)(2,1)S(1)} all-gather(bf16[256,192]{0,1:T(8,128)(2,1)S(1)} %copy-done.4), channel_id=1, replica_groups=mesh['sp'=8,'tp'=4] {'sp'}, dimensions={0}, use_global_device_ids=true | all-gather | bytes 884736 | tf_op jit(solution)/shard_map/all_gather | solution.py:70
  140.2 28.3 %all_gather.40 = bf16[2048,192]{0,1:T(8,128)(2,1)} all-gather(bf16[256,192]{0,1:T(8,128)(2,1)S(1)} %copy-done.5), channel_id=1, replica_groups=mesh['sp'=8,'tp'=4] {'sp'}, dimensions={0}, use_global_device_ids=true | all-gather | bytes 884736 | tf_op jit(solution)/shard_map/all_gather | solution.py:71
  168.4 26.7 %all_gather.48 = bf16[2048,192]{0,1:T(8,128)(2,1)S(1)} all-gather(bf16[256,192]{0,1:T(8,128)(2,1)S(1)} %copy-done.6), channel_id=1, replica_groups=mesh['sp'=8,'tp'=4] {'sp'}, dimensions={0}, use_global_device_ids=true | all-gather | bytes 884736 | tf_op jit(solution)/shard_map/all_gather | solution.py:72
  195.1 26.2 %all_gather.45 = bf16[192,2048]{1,0:T(8,128)(2,1)S(1)} all-gather(bf16[192,256]{1,0:T(8,128)(2,1)S(1)} %copy-done.7), channel_id=1, replica_groups=mesh['sp'=8,'tp'=4] {'sp'}, dimensions={1}, use_global_device_ids=true | all-gather | bytes 884736 | tf_op jit(solution)/shard_map/all_gather | solution.py:187
  221.3 28.5 %all_gather.51 = bf16[192,2048]{1,0:T(8,128)(2,1)} all-gather(bf16[192,256]{1,0:T(8,128)(2,1)S(1)} %copy-done.8), channel_id=1, replica_groups=mesh['sp'=8,'tp'=4] {'sp'}, dimensions={1}, use_global_device_ids=true | all-gather | bytes 884736 | tf_op jit(solution)/shard_map/all_gather | solution.py:188
  249.8 1.8 convolution_convert_fusion.2
  251.6 26.4 %all_gather.47 = bf16[2048,64]{0,1:T(8,128)(2,1)} all-gather(bf16[256,64]{0,1:T(8,128)(2,1)S(1)} %convolution_convert_fusion.2), channel_id=1, replica_groups=mesh['sp'=8,'tp'=4] {'sp'}, dimensions={0}, use_global_device_ids=true | all-gather | bytes 294912 | tf_op jit(solution)/shard_map/all_gather | solution.py:141
  278.0 1.7 convolution_convert_fusion.1
  279.7 27.0 %all_gather.50 = bf16[2048,64]{0,1:T(8,128)(2,1)} all-gather(bf16[256,64]{0,1:T(8,128)(2,1)S(1)} %convolution_convert_fusion.1), channel_id=1, replica_groups=mesh['sp'=8,'tp'=4] {'sp'}, dimensions={0}, use_global_device_ids=true | all-gather | bytes 294912 | tf_op jit(solution)/shard_map/all_gather | solution.py:142
  306.7 1.7 fusion.56
  310.0 25.3 %all_gather.44 = bf16[8,3,4096]{2,1,0:T(4,128)(2,1)S(1)} all-gather(bf16[1,3,4096]{2,1,0:T(4,128)(2,1)S(1)} %add_convert_fusion.1), channel_id=1, replica_groups=mesh['sp'=8,'tp'=4] {'sp'}, dimensions={0}, use_global_device_ids=true | all-gather | bytes 221184 | tf_op jit(solution)/shard_map/all_gather | solution.py:105
  337.2 3.4 while.10
  337.3 3.0 conditional.3
  338.1 1.2 fusion.55
  339.3 1.0 fusion.6
  341.8 1.4 fusion.16
  343.3 112.0 %reduce-scatter.2.cloned.1.call-done = bf16[64,2048]{1,0:T(8,128)(2,1)} async-done(((bf16[256,2048]{1,0:T(8,128)(2,1)}), bf16[64,2048]{1,0:T(8,128)(2,1)}) %reduce-scatter.2.cloned.1.call-update) | async-done | bytes 262160 | tf_op jit(solution)/shard_map/reduce_scatter | solution.py:190
  (99 shorter events, 9.5 us)
Async XLA Ops:
  6.5 24.4 %copy-start.9 = (bf16[256,64]{0,1:T(8,128)(2,1)S(1)}, bf16[256,64]{0,1:T(8,128)(2,1)}, u32[]{:S(2)}) copy-start(bf16[256,64]{0,1:T(8,128)(2,1)} %param.22) | copy-start | bytes 98308
  6.5 51.3 %copy-start.10 = (bf16[256,64]{0,1:T(8,128)(2,1)S(1)}, bf16[256,64]{0,1:T(8,128)(2,1)}, u32[]{:S(2)}) copy-start(bf16[256,64]{0,1:T(8,128)(2,1)} %param.23) | copy-start | bytes 98308
  6.5 77.7 %copy-start.3 = (bf16[256,192]{0,1:T(8,128)(2,1)S(1)}, bf16[256,192]{0,1:T(8,128)(2,1)}, u32[]{:S(2)}) copy-start(bf16[256,192]{0,1:T(8,128)(2,1)} %param.18) | copy-start | bytes 294916
  6.5 105.3 %copy-start.4 = (bf16[256,192]{0,1:T(8,128)(2,1)S(1)}, bf16[256,192]{0,1:T(8,128)(2,1)}, u32[]{:S(2)}) copy-start(bf16[256,192]{0,1:T(8,128)(2,1)} %param.19) | copy-start | bytes 294916
  6.5 243.2 %all-gather.3.cloned.1.call-start = ((), (), s32[]{:S(2)}) async-start(), calls=%async_computation.1 | async-start | bytes 1310720 | tf_op jit(solution)/shard_map/all_gather | solution.py:59
  9.6 130.6 %copy-start.5 = (bf16[256,192]{0,1:T(8,128)(2,1)S(1)}, bf16[256,192]{0,1:T(8,128)(2,1)}, u32[]{:S(2)}) copy-start(bf16[256,192]{0,1:T(8,128)(2,1)} %param.20) | copy-start | bytes 294916
  9.6 445.7 %reduce-scatter.2.cloned.1.call-start = ((), (), s32[]{:S(2)}) async-start(), calls=%async_computation.2 | async-start | bytes 1310720 | tf_op jit(solution)/shard_map/reduce_scatter | solution.py:190
  11.7 156.7 %copy-start.6 = (bf16[256,192]{0,1:T(8,128)(2,1)S(1)}, bf16[256,192]{0,1:T(8,128)(2,1)}, u32[]{:S(2)}) copy-start(bf16[256,192]{0,1:T(8,128)(2,1)} %param.21) | copy-start | bytes 294916
  31.0 164.1 %copy-start.7 = (bf16[192,256]{1,0:T(8,128)(2,1)S(1)}, bf16[192,256]{1,0:T(8,128)(2,1)}, u32[]{:S(2)}) copy-start(bf16[192,256]{1,0:T(8,128)(2,1)} %param.24) | copy-start | bytes 294916
  84.2 137.0 %copy-start.8 = (bf16[192,256]{1,0:T(8,128)(2,1)S(1)}, bf16[192,256]{1,0:T(8,128)(2,1)}, u32[]{:S(2)}) copy-start(bf16[192,256]{1,0:T(8,128)(2,1)} %param.25) | copy-start | bytes 294916
  249.8 57.0 %copy-start = (bf16[256,2048]{1,0:T(8,128)(2,1)S(1)}, bf16[256,2048]{1,0:T(8,128)(2,1)}, u32[]{:S(2)}) copy-start(bf16[256,2048]{1,0:T(8,128)(2,1)} %all-gather.3.cloned.1.call-done) | copy-start | bytes 3145732
  306.7 2.3 copy-start.1
  309.0 0.9 copy-start.12
  309.0 26.8 %copy-start.11 = (f32[3,256]{1,0:T(4,128)S(1)}, f32[3,256]{1,0:T(4,128)}, u32[]{:S(2)}) copy-start(f32[3,256]{1,0:T(4,128)} %bitcast_add_fusion.2) | copy-start | bytes 9220
  340.7 1.1 copy-start.2
Sparse Core Ops, SparseCore 0:
  9.7 19.1 all-gather.2
  343.4 111.8 reduce-scatter.1
where the time goes:
time: 465 us; the launch traced here: 462 us
  blocking collectives  314 us (68%)
  waiting for transfers between devices  112 us (24%)
  between operations  13.7 us (3%)
  matrix products  12.1 us (3%)
  other arithmetic  6.14 us (1%)
    reduce_scatter x1, waiting for transfers between devices, body(): lax.psum_scatter((jnp.dot(retained, out_ret, preferred_element_type=jnp.f...  112 us
    all_gather x1, blocking collectives, body(): lax.all_gather(w_out_att, 'sp', axis=1, tiled=True)  28.5 us
    all_gather x1, blocking collectives, body(): lax.all_gather(w_value_ret, 'sp', axis=0, tiled=True)  28.3 us
    all_gather x1, blocking collectives, body(): lax.all_gather(w_query_ret, 'sp', axis=0, tiled=True)  27.6 us
    all_gather x1, blocking collectives, body(): value_piece = lax.all_gather(value_rows, 'sp', axis=0, tiled=True)  27 us
    all_gather x1, blocking collectives, body(): lax.all_gather(w_key_att, 'sp', axis=0, tiled=True)  26.9 us
    all_gather x1, blocking collectives, body(): lax.all_gather(w_query_att, 'sp', axis=0, tiled=True)  26.7 us
    all_gather x1, blocking collectives, body(): lax.all_gather(w_key_ret, 'sp', axis=0, tiled=True)  26.6 us
  transfers between devices with their start and end apart: 2, of which 1 were waited for; matrix products, arithmetic and copies ran while one was open for 1% of the time, Pallas kernels for 0%

commit v1 on v0

--- a/solution.py
+++ b/solution.py
@@ -1,16 +1,417 @@
+import functools
+
 import jax
 import jax.numpy as jnp
 from jax import lax
+from jax.experimental import pallas as pl
+from jax.experimental.pallas import tpu as pltpu
 from jax.sharding import PartitionSpec as P
 
 HEAD = 64
+EPS = 1e-06
+THETA = 10000.0
+F32 = jnp.float32
+BF16 = jnp.bfloat16
+MESH = pl.DeviceIdType.MESH
 SPAN = 256
 KEY_SPAN = 256
-
-
-EPS = 1e-06
-THETA = 10000.0
+LANES = 128
 HIGH = lax.Precision.HIGHEST
+
+
+def ring_to_sp(place, n):
+    if n % 2:
+        return place
+    back = place // (n // 2)
+    return (1 - back) * 2 * place + back * (2 * (n - 1 - place) + 1)
+
+
+def sp_to_ring(index, n):
+    if n % 2:
+        return index
+    odd, pair = index % 2, index // 2
+    return (1 - odd) * pair + odd * (n - 1 - pair)
+
+
+def dot(a, b, dims=((1,), (0,))):
+    return lax.dot_general(a, b, (dims, ((), ())), preferred_element_type=F32)
+
+
+def kernel(
+    n,
+    m,
+    heads,
+    chunks,
+    tok_ref,
+    gain_ref,
+    wa_ref,
+    wb_ref,
+    wo_ref,
+    cos_ref,
+    sin_ref,
+    within_ref,
+    turned_ref,
+    gate_col_ref,
+    gate_ref,
+    out_ref,
+    xbuf,
+    abuf,
+    bbuf,
+    obuf,
+    kvbuf,
+    state,
+    num,
+    den,
+    outbuf,
+    rsbuf,
+    *sems,
+):
+    (x_send, x_recv, a_send, a_recv, b_send, b_recv, o_send, o_recv, kv_send, kv_recv, r_send,
+     r_recv) = sems
+    me = lax.axis_index("sp")
+    mine = lax.axis_index("tp")
+    place = sp_to_ring(me, n)
+    right = ring_to_sp((place + 1) % n, n)
+    left = ring_to_sp((place + n - 1) % n, n)
+    tok = xbuf.shape[0]
+    rows = tok // m
+    width = heads * HEAD
+
+    barrier = pltpu.get_barrier_semaphore()
+    for r in range(1, n):
+        pl.semaphore_signal(barrier, inc=1, device_id={"sp": (me + r) % n}, device_id_type=MESH)
+    for r in range(1, m):
+        pl.semaphore_signal(barrier, inc=1, device_id={"tp": (mine + r) % m}, device_id_type=MESH)
+
+    abuf[me] = wa_ref[...]
+    bbuf[me] = wb_ref[...]
+    obuf[me] = wo_ref[...]
+    values = tok_ref[...].astype(F32)
+    scale = lax.rsqrt(jnp.mean(values * values, axis=-1, keepdims=True) + EPS)
+    own = pl.ds(mine * rows, rows)
+    xbuf[own, :] = (values * scale * gain_ref[...]).astype(BF16)
+    pl.semaphore_wait(barrier, n - 1 + m - 1)
+
+    def ring_copy(own_ref, buf, send, recv, step, way, chunk):
+        owner = ring_to_sp((place + (n - step if way == 0 else step)) % n, n)
+        half = buf.shape[1] // 2
+        piece = half // chunks
+        span = pl.ds(way * half + chunk * piece, piece)
+        source = own_ref.at[span] if step == 0 else buf.at[owner, span]
+        return pltpu.make_async_remote_copy(
+            src_ref=source,
+            dst_ref=buf.at[owner, span],
+            send_sem=send.at[way, step, chunk],
+            recv_sem=recv.at[way, step, chunk],
+            device_id={"sp": right if way == 0 else left},
+            device_id_type=MESH,
+        )
+
+    def ring_wait(own_ref, buf, send, recv, step, way, chunk):
+        source = ring_to_sp((place + (n - step - 1 if way == 0 else step + 1)) % n, n)
+        half = buf.shape[1] // 2
+        piece = half // chunks
+        span = pl.ds(way * half + chunk * piece, piece)
+        pltpu.make_async_remote_copy(
+            src_ref=buf.at[source, span],
+            dst_ref=buf.at[source, span],
+            send_sem=send.at[way, step, chunk],
+            recv_sem=recv.at[way, step, chunk],
+            device_id={"sp": right if way == 0 else left},
+            device_id_type=MESH,
+        ).wait_recv()
+
+    started = []
+
+    def ring_step(group, step):
+        for chunk in range(chunks):
+            for way in range(2):
+                if step > 0:
+                    ring_wait(*group, step - 1, way, chunk)
+                if step < n - 1:
+                    copy = ring_copy(*group, step, way, chunk)
+                    copy.start()
+                    started.append(copy)
+
+    ring_a = (wa_ref, abuf, a_send, a_recv)
+    ring_b = (wb_ref, bbuf, b_send, b_recv)
+    ring_o = (wo_ref, obuf, o_send, o_recv)
+
+    x_copies = []
+    for r in range(1, m):
+        copy = pltpu.make_async_remote_copy(
+            src_ref=xbuf.at[own],
+            dst_ref=xbuf.at[own],
+            send_sem=x_send.at[r - 1],
+            recv_sem=x_recv.at[r - 1],
+            device_id={"tp": (mine + r) % m},
+            device_id_type=MESH,
+        )
+        copy.start()
+        started.append(copy)
+    for step in range(n - 1):
+        ring_step(ring_a, step)
+    ring_step(ring_b, 0)
+    for r in range(1, m):
+        other = pl.ds(((mine + m - r) % m) * rows, rows)
+        pltpu.make_async_remote_copy(
+            src_ref=xbuf.at[other],
+            dst_ref=xbuf.at[other],
+            send_sem=x_send.at[r - 1],
+            recv_sem=x_recv.at[r - 1],
+            device_id={"tp": (mine + r) % m},
+            device_id_type=MESH,
+        ).wait_recv()
+    ring_step(ring_a, n - 1)
+
+    cosine, sine = cos_ref[...], sin_ref[...]
+
+    def rope(field):
+        half = HEAD // 2
+        first, second = field[:, :half], field[:, half:]
+        return jnp.concatenate(
+            [first * cosine - second * sine, first * sine + second * cosine], axis=-1
+        )
+
+    proj = dot(xbuf[...], abuf[...].reshape(-1, abuf.shape[2]))
+    pair = proj[:, : 2 * HEAD].astype(BF16)
+    within = within_ref[...]
+    keys, vals, updates, marks = [], [], [], []
+    for h in range(heads):
+        base = 2 * HEAD + h * HEAD
+        key = rope(proj[:, base : base + HEAD]).astype(BF16)
+        val = proj[:, base + width : base + width + HEAD].astype(BF16)
+        column = within[:, h : h + 1]
+        last = column[tok - 1 :, :]
+        faded = (key.astype(F32) * jnp.exp(last - column)).astype(BF16)
+        updates.append(dot(faded, val, ((0,), (0,))))
+        high = last.astype(BF16).astype(F32)
+        low = last - high
+        marks.append(jnp.broadcast_to(high, (8, HEAD)))
+        marks.append(jnp.broadcast_to(low, (8, HEAD)))
+        keys.append(key)
+        vals.append(val)
+    kvbuf[me, :tok, :] = pair
+    for h in range(heads):
+        kvbuf[me, tok + h * HEAD : tok + (h + 1) * HEAD, :HEAD] = updates[h].astype(BF16)
+    kvbuf[me, tok : tok + 16 * heads, HEAD:] = jnp.concatenate(marks, axis=0).astype(BF16)
+    for d in range(1, n):
+        def send_kv(d=d):
+            pltpu.make_async_remote_copy(
+                src_ref=kvbuf.at[me],
+                dst_ref=kvbuf.at[me],
+                send_sem=kv_send.at[d],
+                recv_sem=kv_recv.at[me],
+                device_id={"sp": jnp.int32(d)},
+                device_id_type=MESH,
+            ).start()
+
+        pl.when(me < d)(send_kv)
+
+    for step in range(1, n - 1):
+        ring_step(ring_b, step)
+    ring_step(ring_o, 0)
+    ring_step(ring_b, n - 1)
+
+    projq = dot(xbuf[...], bbuf[...].reshape(-1, bbuf.shape[2]))
+    ring_step(ring_o, 1)
+    lines = lax.broadcasted_iota(jnp.int32, (tok, tok), 0)
+    across = lax.broadcasted_iota(jnp.int32, (tok, tok), 1)
+    causal = lines >= across
+    turned = turned_ref[...]
+    local, lifts = [], []
+    for h in range(heads):
+        base = width + h * HEAD
+        query = (rope(projq[:, base : base + HEAD]) * HEAD ** (-0.5)).astype(BF16)
+        column = within[:, h : h + 1]
+        gap = jnp.where(causal, column - turned[h : h + 1, :], 0.0)
+        scores = dot(query, keys[h], ((1,), (1,)))
+        weights = jnp.where(causal, scores * jnp.exp(gap), 0.0).astype(BF16)
+        local.append(dot(weights, vals[h]))
+        lifts.append((query.astype(F32) * jnp.exp(column)).astype(BF16))
+    ring_step(ring_o, 2)
+
+    queries = [
+        (projq[:, h * HEAD : (h + 1) * HEAD] * HEAD ** (-0.5)).astype(BF16) for h in range(heads)
+    ]
+    gate_col = gate_col_ref[...]
+
+    def attend(index, masked):
+        block = kvbuf[index, :tok, :]
+        key, val = block[:, :HEAD], block[:, HEAD:]
+        gates = gate_ref[:, pl.ds(pl.multiple_of(index * tok, tok), tok)]
+        for h in range(heads):
+            logits = dot(queries[h], key, ((1,), (1,)))
+            logits = logits + gate_col[:, h : h + 1] - gates[h : h + 1, :]
+            if masked:
+                logits = jnp.where(causal, logits, -jnp.inf)
+            weights = jnp.exp(logits)
+            den[h] += jnp.broadcast_to(jnp.sum(weights, axis=-1, keepdims=True), (tok, HEAD))
+            num[h] += dot(weights.astype(BF16), val)
+
+    den[...] = jnp.zeros_like(den)
+    num[...] = jnp.zeros_like(num)
+    state[...] = jnp.zeros_like(state)
+    attend(me, True)
+    for j in range(n - 1):
+        def earlier(j=j):
+            pltpu.make_async_remote_copy(
+                src_ref=kvbuf.at[j],
+                dst_ref=kvbuf.at[j],
+                send_sem=kv_send.at[0],
+                recv_sem=kv_recv.at[j],
+                device_id={"sp": right},
+                device_id_type=MESH,
+            ).wait_recv()
+            for h in range(heads):
+                mark = kvbuf[j, tok + 16 * h : tok + 16 * (h + 1), HEAD:].astype(F32)
+                total = mark[0:1] + mark[8:9]
+                new = kvbuf[j, tok + h * HEAD : tok + (h + 1) * HEAD, :HEAD].astype(F32)
+                state[h] = jnp.exp(total) * state[h] + new
+            attend(jnp.int32(j), False)
+
+        pl.when(me > j)(earlier)
+        if 3 + j <= n - 1:
+            ring_step(ring_o, 3 + j)
+    for step in range(3 + n - 1, n):
+        ring_step(ring_o, step)
+
+    retained, attended = [], []
+    for h in range(heads):
+        raw = local[h] + dot(lifts[h], state[h].astype(BF16))
+        centre = jnp.mean(raw, axis=-1, keepdims=True)
+        spread = jnp.mean(jnp.square(raw - centre), axis=-1, keepdims=True)
+        retained.append(((raw - centre) * lax.rsqrt(spread + EPS)).astype(BF16))
+        attended.append((num[h] / den[h]).astype(BF16))
+    mixed = jnp.concatenate(retained + attended, axis=-1)
+
+    def out_copy(r, part, span):
+        return pltpu.make_async_remote_copy(
+            src_ref=outbuf.at[(mine + r) % m, :, span],
+            dst_ref=rsbuf.at[mine, :, span],
+            send_sem=r_send.at[r - 1, part],
+            recv_sem=r_recv.at[r - 1, part],
+            device_id={"tp": (mine + r) % m},
+            device_id_type=MESH,
+        )
+
+    columns = obuf.shape[2]
+    group = 2 if n % 2 == 0 else 1
+    for part in range(n // group):
+        for k in range(part * group, part * group + group):
+            share = dot(mixed, obuf[k]).astype(BF16)
+            outbuf[:, :, k * columns : (k + 1) * columns] = share.reshape(m, rows, columns)
+        span = pl.ds(part * group * columns, group * columns)
+        for r in range(1, m):
+            copy = out_copy(r, part, span)
+            copy.start()
+            started.append(copy)
+    for part in range(n // group):
+        span = pl.ds(part * group * columns, group * columns)
+        total = outbuf[mine, :, span].astype(F32)
+        for r in range(1, m):
+            other = (mine + m - r) % m
+            pltpu.make_async_remote_copy(
+                src_ref=rsbuf.at[other, :, span],
+                dst_ref=rsbuf.at[other, :, span],
+                send_sem=r_send.at[r - 1, part],
+                recv_sem=r_recv.at[r - 1, part],
+                device_id={"tp": (mine + r) % m},
+                device_id_type=MESH,
+            ).wait_recv()
+            total = total + rsbuf[other, :, span].astype(F32)
+        out_ref[:, span] = total.astype(BF16)
+
+    for copy in started:
+        copy.wait_send()
+    for d in range(1, n):
+        def sent(d=d):
+            pltpu.make_async_remote_copy(
+                src_ref=kvbuf.at[me],
+                dst_ref=kvbuf.at[me],
+                send_sem=kv_send.at[d],
+                recv_sem=kv_recv.at[me],
+                device_id={"sp": jnp.int32(d)},
+                device_id_type=MESH,
+            ).wait_send()
+
+        pl.when(me < d)(sent)
+
+
+def body(
+    n,
+    m,
+    tokens,
+    pre_gain,
+    w_query_ret,
+    w_key_ret,
+    w_value_ret,
+    w_query_att,
+    w_key_att,
+    w_value_att,
+    w_out_ret,
+    w_out_att,
+    retain_log,
+    forget_total,
+):
+    rows, depth = tokens.shape
+    tok = rows * m
+    heads = retain_log.shape[1]
+    offset = lax.axis_index("sp") * tok
+    wa = jnp.concatenate([w_key_att, w_value_att, w_key_ret, w_value_ret], axis=1)
+    wb = jnp.concatenate([w_query_att, w_query_ret], axis=1)
+    wo = jnp.concatenate([w_out_ret, w_out_att], axis=0)
+    half = HEAD // 2
+    positions = (offset + jnp.arange(tok, dtype=jnp.int32)).astype(F32)
+    inverse = THETA ** (-jnp.arange(half, dtype=F32) / half)
+    angles = positions[:, None] * inverse[None, :]
+    within = jnp.cumsum(retain_log, axis=0)
+    gate_col = lax.dynamic_slice_in_dim(forget_total, offset, tok, 1).T
+    chunks = 4
+    vmem = pl.BlockSpec(memory_space=pltpu.VMEM)
+    dma = pltpu.SemaphoreType.DMA
+    rings = [dma((2, n - 1, chunks))] * 6
+    parts = n // 2 if n % 2 == 0 else n
+    return pl.pallas_call(
+        functools.partial(kernel, n, m, heads, chunks),
+        out_shape=jax.ShapeDtypeStruct((rows, depth), BF16),
+        in_specs=[vmem] * 11,
+        out_specs=vmem,
+        scratch_shapes=[
+            pltpu.VMEM((tok, depth), BF16),
+            pltpu.VMEM((n,) + wa.shape, BF16),
+            pltpu.VMEM((n,) + wb.shape, BF16),
+            pltpu.VMEM((n,) + wo.shape, BF16),
+            pltpu.VMEM((n, tok + heads * HEAD, 2 * HEAD), BF16),
+            pltpu.VMEM((heads, HEAD, HEAD), F32),
+            pltpu.VMEM((heads, tok, HEAD), F32),
+            pltpu.VMEM((heads, tok, HEAD), F32),
+            pltpu.VMEM((m, rows, depth), BF16),
+            pltpu.VMEM((m, rows, depth), BF16),
+            dma((m - 1,)),
+            dma((m - 1,)),
+            *rings,
+            dma((n,)),
+            dma((n,)),
+            dma((m - 1, parts)),
+            dma((m - 1, parts)),
+        ],
+        compiler_params=pltpu.CompilerParams(
+            collective_id=0, has_side_effects=True, vmem_limit_bytes=60 * 1024 * 1024
+        ),
+    )(
+        tokens,
+        pre_gain[None, :],
+        wa,
+        wb,
+        wo,
+        jnp.cos(angles),
+        jnp.sin(angles),
+        within,
+        within.T,
+        gate_col,
+        forget_total,
+    )
 
 
 def rotate(field, positions):
@@ -38,7 +439,7 @@
     return (jnp.exp(decay)[:, None, None] * state + update, state)
 
 
-def body(
+def plain_body(
     tokens,
     pre_gain,
     w_query_ret,
@@ -198,9 +599,17 @@
     )
 
 
+def choose(n, m, *arrays):
+    tokens, w_key_ret, w_out_ret = arrays[0], arrays[3], arrays[8]
+    whole_tiles = w_out_ret.shape[1] % LANES == 0 and w_key_ret.shape[0] % LANES == 0
+    if whole_tiles and tokens.shape[0] * m == SPAN and arrays[7].shape[1] == HEAD:
+        return body(n, m, *arrays)
+    return plain_body(*arrays)
+
+
 def solution(mesh):
     return jax.shard_map(
-        body,
+        functools.partial(choose, mesh.shape["sp"], mesh.shape["tp"]),
         mesh=mesh,
         in_specs=(
             P(("sp", "tp"), None),

time: 465 us -> 117 us (0.25)
  blocking collectives: 314 us -> 0 us
  waiting for transfers between devices: 112 us -> 0 us
  Pallas kernels: 0 us -> 104 us
  between operations: 13.7 us -> 0.1 us
  matrix products: 12.1 us -> 0 us
    all_gather x12 -> x0, blocking collectives: 314 us -> none  [the longest x1 28.5 us: body(): lax.all_gather(w_out_att, 'sp', axis=1, tiled=True)]
    reduce_scatter x1 -> x0, waiting for transfers between devices: 112 us -> none  [body(): lax.psum_scatter((jnp.dot(retained, out_ret, preferred_element_type=jnp.f...]
    pallas_call x0 -> x1, Pallas kernels: none -> 104 us  [body(): pl.pallas_call(functools.partial(kernel, n, m, heads, chunks), out_shape=...]
    dot_general x14 -> x0, matrix products: 12.1 us -> none  [the longest x6 6.75 us: body(): jnp.dot(gathered, piece, preferred_element_type=jnp.float32)]
    unnamed x27 -> x29, local copies, waits for them, and re-layouts: 0.69 us -> 6.25 us
  transfers between devices with their start and end apart: 2 -> 0, of which waited for: 1 -> 0; matrix products, arithmetic and copies ran while one was open for 1% -> 0% of each run, Pallas kernels for 0% -> 0%
where the time goes in v1:
time: 117 us
  Pallas kernels  104 us (89%)
  local copies, waits for them, and re-layouts  8.04 us (7%)
  other arithmetic  4.57 us (4%)
    pallas_call x1, Pallas kernels, body(): pl.pallas_call(functools.partial(kernel, n, m, heads, chunks), out_shape=...  104 us
    unnamed x29, local copies, waits for them, and re-layouts  6.25 us

profile of v1, /device:TPU:1, one launch (start us, length us, event | category | flops | bytes accessed | tf_op | source)
XLA Modules:
  0.0 116.8 jit_solution(11708786644750952668)
XLA Ops:
  0.0 0.7 copy-done.9
  0.7 0.9 reduce-window.6
  1.7 0.1 copy.30
  1.8 0.1 copy.31
  2.0 0.7 constant_dynamic-slice_fusion
  2.7 0.1 copy.23
  2.8 0.6 copy-done.8
  3.5 0.1 copy.24
  3.6 0.8 copy.34
  4.4 0.8 copy.33.within_ref
  5.2 0.1 copy-done
  5.3 0.1 copy.28
  5.4 0.8 copy-done.1
  6.2 0.1 copy.25
  6.3 0.8 copy-done.2
  7.1 0.1 copy.26
  7.2 0.8 pad_maximum_fusion.wa_ref
  8.1 0.1 copy.27
  8.2 0.8 pad_maximum_fusion.1.wb_ref
  9.0 0.1 copy-done.4
  9.1 0.7 pad_maximum_fusion.2.wo_ref
  9.8 1.2 %multiply_sine_fusion = (f32[256,32]{1,0:T(8,128)}, f32[256,32]{1,0:T(8,128)}) fusion(f32[256]{0:T(256)S(1)} %add_convert_fusion, f32[32]{0:T(128)S(1)} %multiply_power_fusion), kind=kLoop, calls=%fused_computation.3 | loop fusion | flops 8192 | bytes 66688 | tf_op jit(solution)/shard_map/sin | solution.py:409
  11.0 104.1 %shard_map.118 = bf16[64,2048]{1,0:T(8,128)(2,1)} custom-call(bf16[64,2048]{1,0:T(8,128)(2,1)} %tok_ref.1, f32[1,2048]{1,0:T(1,128)} %bitcast.16, bf16[256,512]{1,0:T(8,128)(2,1)} %pad_maximum_fusion.wa_ref, bf16[256,384]{1,0:T(8,128)(2,1)} %pad_maximum_fusion.1.wb_ref, bf16[384,256]{1,0:T(8,128)(2,1)} %pad_maximum_fusion.2.wo_ref, ...), custom_call_target="tpu_custom_call" | custom-call | tf_op jit(solution)/shard_map/pallas_call | solution.py:375
  115.1 1.7 %copy.41 = bf16[64,2048]{1,0:T(8,128)(2,1)} copy(bf16[64,2048]{1,0:T(8,128)(2,1)} %shard_map.118) | data formatting | bytes 524288
  (22 shorter events, 0.3 us)
Async XLA Ops:
  0.0 0.7 copy-start.9
  0.0 2.7 %copy-start.7 = (bf16[256,64]{0,1:T(8,128)(2,1)S(1)}, bf16[256,64]{0,1:T(8,128)(2,1)}, u32[]{:S(2)}) copy-start(bf16[256,64]{0,1:T(8,128)(2,1)} %param.18) | copy-start | bytes 98308
  2.0 2.4 %copy-start.6 = (f32[1,3,2,128]{3,1,2,0:T(4,128)}, f32[1,3,2,128]{3,1,2,0:T(4,128)S(1)}, u32[]{:S(2)}) copy-start(f32[1,3,2,128]{3,1,2,0:T(4,128)S(1)} %copy.39) | copy-start | bytes 9220
  2.7 0.8 copy-start.8
  4.4 0.9 copy-start
  5.3 0.9 copy-start.1
  6.2 0.9 copy-start.2
  7.2 0.9 copy-start.3
  8.2 0.9 copy-start.4
  8.2 0.9 copy-start.5

commit v2 on v1

--- a/solution.py
+++ b/solution.py
@@ -2,6 +2,7 @@
 
 import jax
 import jax.numpy as jnp
+import numpy as np
 from jax import lax
 from jax.experimental import pallas as pl
 from jax.experimental.pallas import tpu as pltpu
@@ -16,6 +17,7 @@
 SPAN = 256
 KEY_SPAN = 256
 LANES = 128
+CHUNKS = (4, 4, 4, 2)
 HIGH = lax.Precision.HIGHEST
 
 
@@ -42,18 +44,28 @@
     m,
     heads,
     chunks,
-    tok_ref,
+    tok_hbm,
     gain_ref,
-    wa_ref,
-    wb_ref,
-    wo_ref,
-    cos_ref,
-    sin_ref,
-    within_ref,
-    turned_ref,
-    gate_col_ref,
+    wq_ret_hbm,
+    wk_ret_hbm,
+    wv_ret_hbm,
+    wq_att_hbm,
+    wk_att_hbm,
+    wv_att_hbm,
+    wo_ret_hbm,
+    wo_att_hbm,
+    table_hbm,
+    logs_ref,
     gate_ref,
     out_ref,
+    tokens,
+    wq_ret,
+    wk_ret,
+    wv_ret,
+    wq_att,
+    wk_att,
+    wv_att,
+    table,
     xbuf,
     abuf,
     bbuf,
@@ -66,7 +78,7 @@
     rsbuf,
     *sems,
 ):
-    (x_send, x_recv, a_send, a_recv, b_send, b_recv, o_send, o_recv, kv_send, kv_recv, r_send,
+    (load, x_send, x_recv, a_send, a_recv, b_send, b_recv, o_send, o_recv, k_send, k_recv, r_send,
      r_recv) = sems
     me = lax.axis_index("sp")
     mine = lax.axis_index("tp")
@@ -77,29 +89,47 @@
     rows = tok // m
     width = heads * HEAD
 
+    half_o = wo_ret_hbm.shape[0]
+    loads = [
+        pltpu.make_async_copy(source, target, load.at[k])
+        for k, (source, target) in enumerate((
+            (wk_att_hbm, wk_att),
+            (wv_att_hbm, wv_att),
+            (wk_ret_hbm, wk_ret),
+            (wv_ret_hbm, wv_ret),
+            (tok_hbm, tokens),
+            (wq_att_hbm, wq_att),
+            (wq_ret_hbm, wq_ret),
+            (table_hbm.at[pl.ds(pl.multiple_of(me * tok, tok), tok)], table),
+            (wo_ret_hbm, obuf.at[me, pl.ds(0, half_o)]),
+            (wo_att_hbm, obuf.at[me, pl.ds(half_o, wo_att_hbm.shape[0])]),
+        ))
+    ]
+    for copy in loads:
+        copy.start()
+
     barrier = pltpu.get_barrier_semaphore()
-    for r in range(1, n):
-        pl.semaphore_signal(barrier, inc=1, device_id={"sp": (me + r) % n}, device_id_type=MESH)
+    for other in (left, right):
+        pl.semaphore_signal(barrier, inc=1, device_id={"sp": other}, device_id_type=MESH)
     for r in range(1, m):
         pl.semaphore_signal(barrier, inc=1, device_id={"tp": (mine + r) % m}, device_id_type=MESH)
 
-    abuf[me] = wa_ref[...]
-    bbuf[me] = wb_ref[...]
-    obuf[me] = wo_ref[...]
-    values = tok_ref[...].astype(F32)
-    scale = lax.rsqrt(jnp.mean(values * values, axis=-1, keepdims=True) + EPS)
-    own = pl.ds(mine * rows, rows)
-    xbuf[own, :] = (values * scale * gain_ref[...]).astype(BF16)
-    pl.semaphore_wait(barrier, n - 1 + m - 1)
-
-    def ring_copy(own_ref, buf, send, recv, step, way, chunk):
-        owner = ring_to_sp((place + (n - step if way == 0 else step)) % n, n)
+    for copy in loads[:4]:
+        copy.wait()
+    abuf[me, :, :HEAD] = wk_att[...]
+    abuf[me, :, HEAD : 2 * HEAD] = wv_att[...]
+    abuf[me, :, 2 * HEAD : 2 * HEAD + width] = wk_ret[...]
+    abuf[me, :, 2 * HEAD + width :] = wv_ret[...]
+    pl.semaphore_wait(barrier, 2 + m - 1)
+
+    def ring_copy(buf, send, recv, pieces, step, way, chunk, arriving):
+        hops = step + 1 if arriving else step
+        owner = ring_to_sp((place + (n - hops if way == 0 else hops)) % n, n)
         half = buf.shape[1] // 2
-        piece = half // chunks
+        piece = half // pieces
         span = pl.ds(way * half + chunk * piece, piece)
-        source = own_ref.at[span] if step == 0 else buf.at[owner, span]
         return pltpu.make_async_remote_copy(
-            src_ref=source,
+            src_ref=buf.at[owner, span],
             dst_ref=buf.at[owner, span],
             send_sem=send.at[way, step, chunk],
             recv_sem=recv.at[way, step, chunk],
@@ -107,37 +137,29 @@
             device_id_type=MESH,
         )
 
-    def ring_wait(own_ref, buf, send, recv, step, way, chunk):
-        source = ring_to_sp((place + (n - step - 1 if way == 0 else step + 1)) % n, n)
-        half = buf.shape[1] // 2
-        piece = half // chunks
-        span = pl.ds(way * half + chunk * piece, piece)
-        pltpu.make_async_remote_copy(
-            src_ref=buf.at[source, span],
-            dst_ref=buf.at[source, span],
-            send_sem=send.at[way, step, chunk],
-            recv_sem=recv.at[way, step, chunk],
-            device_id={"sp": right if way == 0 else left},
-            device_id_type=MESH,
-        ).wait_recv()
-
     started = []
 
     def ring_step(group, step):
-        for chunk in range(chunks):
+        for chunk in range(group[3]):
             for way in range(2):
                 if step > 0:
-                    ring_wait(*group, step - 1, way, chunk)
+                    ring_copy(*group, step - 1, way, chunk, True).wait_recv()
                 if step < n - 1:
-                    copy = ring_copy(*group, step, way, chunk)
+                    copy = ring_copy(*group, step, way, chunk, False)
                     copy.start()
                     started.append(copy)
 
-    ring_a = (wa_ref, abuf, a_send, a_recv)
-    ring_b = (wb_ref, bbuf, b_send, b_recv)
-    ring_o = (wo_ref, obuf, o_send, o_recv)
-
-    x_copies = []
+    ring_a = (abuf, a_send, a_recv, chunks[0])
+    ring_b = (bbuf, b_send, b_recv, chunks[1])
+    ring_o = (obuf, o_send, o_recv, chunks[2])
+    ring_k = (kvbuf, k_send, k_recv, chunks[3])
+
+    ring_step(ring_a, 0)
+    loads[4].wait()
+    values = tokens[...].astype(F32)
+    scale = lax.rsqrt(jnp.mean(values * values, axis=-1, keepdims=True) + EPS)
+    own = pl.ds(mine * rows, rows)
+    xbuf[own, :] = (values * scale * gain_ref[...]).astype(BF16)
     for r in range(1, m):
         copy = pltpu.make_async_remote_copy(
             src_ref=xbuf.at[own],
@@ -149,7 +171,31 @@
         )
         copy.start()
         started.append(copy)
-    for step in range(n - 1):
+    ring_step(ring_a, 1)
+    for copy in loads[5:]:
+        copy.wait()
+    bbuf[me, :, :width] = wq_att[...]
+    bbuf[me, :, width:] = wq_ret[...]
+    ring_step(ring_a, 2)
+
+    lines = lax.broadcasted_iota(jnp.int32, (tok, tok), 0)
+    across = lax.broadcasted_iota(jnp.int32, (tok, tok), 1)
+    causal = lines >= across
+    upto = jnp.where(lines <= across, 1.0, 0.0)
+    logs = jnp.concatenate([logs_ref[...], jnp.zeros((8 - heads, tok), F32)], axis=0)
+    turned = lax.dot_general(
+        logs, upto, (((1,), (0,)), ((), ())),
+        preferred_element_type=F32, precision=lax.Precision.HIGHEST,
+    )
+    fill = jnp.zeros((LANES - 8, tok), F32)
+    within = jnp.concatenate([turned, fill], axis=0).T
+    gates_own = gate_ref[:, pl.ds(pl.multiple_of(me * tok, tok), tok)]
+    gate_col = jnp.concatenate(
+        [gates_own, jnp.zeros((LANES - heads, tok), F32)], axis=0
+    ).T
+    cosine, sine = table[:, : HEAD // 2], table[:, HEAD // 2 :]
+
+    for step in range(3, n - 1):
         ring_step(ring_a, step)
     ring_step(ring_b, 0)
     for r in range(1, m):
@@ -163,8 +209,7 @@
             device_id_type=MESH,
         ).wait_recv()
     ring_step(ring_a, n - 1)
-
-    cosine, sine = cos_ref[...], sin_ref[...]
+    ring_step(ring_b, 1)
 
     def rope(field):
         half = HEAD // 2
@@ -175,7 +220,6 @@
 
     proj = dot(xbuf[...], abuf[...].reshape(-1, abuf.shape[2]))
     pair = proj[:, : 2 * HEAD].astype(BF16)
-    within = within_ref[...]
     keys, vals, updates, marks = [], [], [], []
     for h in range(heads):
         base = 2 * HEAD + h * HEAD
@@ -192,33 +236,27 @@
         keys.append(key)
         vals.append(val)
     kvbuf[me, :tok, :] = pair
-    for h in range(heads):
-        kvbuf[me, tok + h * HEAD : tok + (h + 1) * HEAD, :HEAD] = updates[h].astype(BF16)
-    kvbuf[me, tok : tok + 16 * heads, HEAD:] = jnp.concatenate(marks, axis=0).astype(BF16)
-    for d in range(1, n):
-        def send_kv(d=d):
-            pltpu.make_async_remote_copy(
-                src_ref=kvbuf.at[me],
-                dst_ref=kvbuf.at[me],
-                send_sem=kv_send.at[d],
-                recv_sem=kv_recv.at[me],
-                device_id={"sp": jnp.int32(d)},
-                device_id_type=MESH,
-            ).start()
-
-        pl.when(me < d)(send_kv)
-
-    for step in range(1, n - 1):
-        ring_step(ring_b, step)
-    ring_step(ring_o, 0)
-    ring_step(ring_b, n - 1)
+    marks.append(jnp.zeros((HEAD - 16 * heads, HEAD), F32))
+    blocks = updates + [jnp.concatenate(marks, axis=0)]
+    if len(blocks) % 2:
+        blocks.append(jnp.zeros((HEAD, HEAD), F32))
+    for k in range(0, len(blocks), 2):
+        both = jnp.concatenate(blocks[k : k + 2], axis=1).astype(BF16)
+        kvbuf[me, tok + k // 2 * HEAD : tok + (k // 2 + 1) * HEAD, :] = both
+
+    def piece_of(index, k):
+        lanes = slice(k % 2 * HEAD, (k % 2 + 1) * HEAD)
+        return kvbuf[index, tok + k // 2 * HEAD : tok + (k // 2 + 1) * HEAD, lanes].astype(F32)
+
+    for step in range(n - 1):
+        ring_step(ring_k, step)
+        if step == n - 2:
+            ring_step(ring_o, 0)
+        if step + 2 <= n - 1:
+            ring_step(ring_b, step + 2)
 
     projq = dot(xbuf[...], bbuf[...].reshape(-1, bbuf.shape[2]))
     ring_step(ring_o, 1)
-    lines = lax.broadcasted_iota(jnp.int32, (tok, tok), 0)
-    across = lax.broadcasted_iota(jnp.int32, (tok, tok), 1)
-    causal = lines >= across
-    turned = turned_ref[...]
     local, lifts = [], []
     for h in range(heads):
         base = width + h * HEAD
@@ -234,7 +272,6 @@
     queries = [
         (projq[:, h * HEAD : (h + 1) * HEAD] * HEAD ** (-0.5)).astype(BF16) for h in range(heads)
     ]
-    gate_col = gate_col_ref[...]
 
     def attend(index, masked):
         block = kvbuf[index, :tok, :]
@@ -253,22 +290,14 @@
     num[...] = jnp.zeros_like(num)
     state[...] = jnp.zeros_like(state)
     attend(me, True)
+    ring_step(ring_k, n - 1)
     for j in range(n - 1):
         def earlier(j=j):
-            pltpu.make_async_remote_copy(
-                src_ref=kvbuf.at[j],
-                dst_ref=kvbuf.at[j],
-                send_sem=kv_send.at[0],
-                recv_sem=kv_recv.at[j],
-                device_id={"sp": right},
-                device_id_type=MESH,
-            ).wait_recv()
+            marked = piece_of(j, heads)
             for h in range(heads):
-                mark = kvbuf[j, tok + 16 * h : tok + 16 * (h + 1), HEAD:].astype(F32)
-                total = mark[0:1] + mark[8:9]
-                new = kvbuf[j, tok + h * HEAD : tok + (h + 1) * HEAD, :HEAD].astype(F32)
-                state[h] = jnp.exp(total) * state[h] + new
-            attend(jnp.int32(j), False)
+                total = marked[16 * h : 16 * h + 1] + marked[16 * h + 8 : 16 * h + 9]
+                state[h] = jnp.exp(total) * state[h] + piece_of(j, h)
+            attend(j, False)
 
         pl.when(me > j)(earlier)
         if 3 + j <= n - 1:
@@ -324,18 +353,6 @@
 
     for copy in started:
         copy.wait_send()
-    for d in range(1, n):
-        def sent(d=d):
-            pltpu.make_async_remote_copy(
-                src_ref=kvbuf.at[me],
-                dst_ref=kvbuf.at[me],
-                send_sem=kv_send.at[d],
-                recv_sem=kv_recv.at[me],
-                device_id={"sp": jnp.int32(d)},
-                device_id_type=MESH,
-            ).wait_send()
-
-        pl.when(me < d)(sent)
 
 
 def body(
@@ -357,42 +374,49 @@
     rows, depth = tokens.shape
     tok = rows * m
     heads = retain_log.shape[1]
-    offset = lax.axis_index("sp") * tok
-    wa = jnp.concatenate([w_key_att, w_value_att, w_key_ret, w_value_ret], axis=1)
-    wb = jnp.concatenate([w_query_att, w_query_ret], axis=1)
-    wo = jnp.concatenate([w_out_ret, w_out_att], axis=0)
     half = HEAD // 2
-    positions = (offset + jnp.arange(tok, dtype=jnp.int32)).astype(F32)
-    inverse = THETA ** (-jnp.arange(half, dtype=F32) / half)
-    angles = positions[:, None] * inverse[None, :]
-    within = jnp.cumsum(retain_log, axis=0)
-    gate_col = lax.dynamic_slice_in_dim(forget_total, offset, tok, 1).T
-    chunks = 4
+    inverse = np.float32(THETA) ** (-np.arange(half, dtype=np.float32) / np.float32(half))
+    angles = np.arange(n * tok, dtype=np.float32)[:, None] * inverse[None, :]
+    table = np.concatenate([np.cos(angles), np.sin(angles)], axis=1).astype(np.float32)
+    chunks = CHUNKS
+    wide_a = 2 * HEAD + 2 * heads * HEAD
+    wide_b = 2 * heads * HEAD
+    deep = w_key_ret.shape[0]
+    deep_o = w_out_ret.shape[0] + w_out_att.shape[0]
+    tall = tok + (heads // 2 + 1) * HEAD
+    hbm = pl.BlockSpec(memory_space=pl.ANY)
     vmem = pl.BlockSpec(memory_space=pltpu.VMEM)
     dma = pltpu.SemaphoreType.DMA
-    rings = [dma((2, n - 1, chunks))] * 6
+    rings = [dma((2, n - 1, c)) for c in chunks for _ in range(2)]
     parts = n // 2 if n % 2 == 0 else n
     return pl.pallas_call(
         functools.partial(kernel, n, m, heads, chunks),
         out_shape=jax.ShapeDtypeStruct((rows, depth), BF16),
-        in_specs=[vmem] * 11,
+        in_specs=[hbm, vmem] + [hbm] * 9 + [vmem] * 2,
         out_specs=vmem,
         scratch_shapes=[
+            pltpu.VMEM(tokens.shape, BF16),
+            pltpu.VMEM(w_query_ret.shape, BF16),
+            pltpu.VMEM(w_key_ret.shape, BF16),
+            pltpu.VMEM(w_value_ret.shape, BF16),
+            pltpu.VMEM(w_query_att.shape, BF16),
+            pltpu.VMEM(w_key_att.shape, BF16),
+            pltpu.VMEM(w_value_att.shape, BF16),
+            pltpu.VMEM((tok, HEAD), F32),
             pltpu.VMEM((tok, depth), BF16),
-            pltpu.VMEM((n,) + wa.shape, BF16),
-            pltpu.VMEM((n,) + wb.shape, BF16),
-            pltpu.VMEM((n,) + wo.shape, BF16),
-            pltpu.VMEM((n, tok + heads * HEAD, 2 * HEAD), BF16),
+            pltpu.VMEM((n, deep, wide_a), BF16),
+            pltpu.VMEM((n, deep, wide_b), BF16),
+            pltpu.VMEM((n, deep_o, w_out_ret.shape[1]), BF16),
+            pltpu.VMEM((n, tall, 2 * HEAD), BF16),
             pltpu.VMEM((heads, HEAD, HEAD), F32),
             pltpu.VMEM((heads, tok, HEAD), F32),
             pltpu.VMEM((heads, tok, HEAD), F32),
             pltpu.VMEM((m, rows, depth), BF16),
             pltpu.VMEM((m, rows, depth), BF16),
+            dma((10,)),
             dma((m - 1,)),
             dma((m - 1,)),
             *rings,
-            dma((n,)),
-            dma((n,)),
             dma((m - 1, parts)),
             dma((m - 1, parts)),
         ],
@@ -402,14 +426,16 @@
     )(
         tokens,
         pre_gain[None, :],
-        wa,
-        wb,
-        wo,
-        jnp.cos(angles),
-        jnp.sin(angles),
-        within,
-        within.T,
-        gate_col,
+        w_query_ret,
+        w_key_ret,
+        w_value_ret,
+        w_query_att,
+        w_key_att,
+        w_value_att,
+        w_out_ret,
+        w_out_att,
+        jnp.asarray(table),
+        retain_log.T,
         forget_total,
     )
 
@@ -602,7 +628,9 @@
 def choose(n, m, *arrays):
     tokens, w_key_ret, w_out_ret = arrays[0], arrays[3], arrays[8]
     whole_tiles = w_out_ret.shape[1] % LANES == 0 and w_key_ret.shape[0] % LANES == 0
-    if whole_tiles and tokens.shape[0] * m == SPAN and arrays[7].shape[1] == HEAD:
+    heads = arrays[10].shape[1]
+    small = 16 * heads <= HEAD and arrays[7].shape[1] == HEAD and arrays[11].shape[0] == heads
+    if whole_tiles and small and tokens.shape[0] * m == SPAN:
         return body(n, m, *arrays)
     return plain_body(*arrays)
 

time: 117 us -> 95.7 us (0.82)
  Pallas kernels: 104 us -> 88 us
  other arithmetic: 4.57 us -> 0 us
    pallas_call x1, Pallas kernels: 104 us -> 88 us  [body(): pl.pallas_call(functools.partial(kernel, n, m, heads, chunks), out_shape=...]
    concatenate x3 -> x0, other arithmetic: 2.3 us -> none  [the longest x1 0.85 us: body(): jnp.concatenate([w_key_att, w_value_att, w_key_ret, w_value_ret], axis=1)]
    sin x1 -> x0, other arithmetic: 1.24 us -> none  [body(): jnp.sin(angles)]
    unnamed x29 -> x17, local copies, waits for them, and re-layouts: 6.25 us -> 7.36 us
where the time goes in v2:
time: 95.7 us; the launch traced here: 95.4 us
  Pallas kernels  88 us (92%)
  local copies, waits for them, and re-layouts  7.36 us (8%)
    pallas_call x1, Pallas kernels, body(): pl.pallas_call(functools.partial(kernel, n, m, heads, chunks), out_shape=...  88 us
    unnamed x17, local copies, waits for them, and re-layouts  7.36 us

profile of v2, /device:TPU:1, one launch (start us, length us, event | category | flops | bytes accessed | tf_op | source)
XLA Modules:
  0.0 95.4 jit_solution(16136757074326413914)
XLA Ops:
  0.0 0.0 copy-start.4
  0.0 0.0 copy-start
  0.0 1.5 %copy.18.wk_att_hbm = bf16[256,64]{1,0:T(8,128)(2,1)} copy(bf16[256,64]{0,1:T(8,128)(2,1)} %param.19) | data formatting | bytes 65536 | tf_op args[6]
  1.5 0.0 copy-done.4
  1.5 0.7 copy.19.wv_att_hbm
  2.3 0.0 copy-done
  2.3 0.0 copy-start.1
  2.3 0.8 copy.14.wq_ret_hbm
  3.0 0.1 copy-done.1
  3.2 0.0 copy-start.2
  3.2 0.8 copy.15.wk_ret_hbm
  3.9 0.1 copy-done.2
  4.0 0.0 copy-start.3
  4.1 0.8 copy.16.wv_ret_hbm
  4.8 0.1 copy-done.3
  4.9 0.8 copy.17.wq_att_hbm
  5.7 88.0 %shard_map.127 = bf16[64,2048]{1,0:T(8,128)(2,1)} custom-call(bf16[64,2048]{1,0:T(8,128)(2,1)} %tok_hbm.1, f32[1,2048]{1,0:T(1,128)} %bitcast.2, bf16[256,192]{1,0:T(8,128)(2,1)} %copy.14.wq_ret_hbm, bf16[256,192]{1,0:T(8,128)(2,1)} %copy.15.wk_ret_hbm, bf16[256,192]{1,0:T(8,128)(2,1)} %copy.16.wv_ret_hbm, bf16[256,192]{1,0:T(8,128)(2,1)} %copy.17.wq_att_hbm, ...), custom_call_target="tpu_custom_call" | custom-call | tf_op jit(solution)/shard_map/pallas_call | solution.py:392
  93.7 1.7 %copy.21 = bf16[64,2048]{1,0:T(8,128)(2,1)} copy(bf16[64,2048]{1,0:T(8,128)(2,1)} %shard_map.127) | data formatting | bytes 524288
Async XLA Ops:
  0.0 1.5 %copy-start.4 = (bf16[256,64]{0,1:T(8,128)(2,1)S(1)}, bf16[256,64]{0,1:T(8,128)(2,1)}, u32[]{:S(2)}) copy-start(bf16[256,64]{0,1:T(8,128)(2,1)} %param.20) | copy-start | bytes 98308
  0.0 2.3 %copy-start = (bf16[256,192]{0,1:T(8,128)(2,1)S(1)}, bf16[256,192]{0,1:T(8,128)(2,1)}, u32[]{:S(2)}) copy-start(bf16[256,192]{0,1:T(8,128)(2,1)} %param.15) | copy-start | bytes 294916
  2.3 0.9 copy-start.1
  3.2 0.9 copy-start.2
  4.0 0.9 copy-start.3

commit v3 on v2

--- a/solution.py
+++ b/solution.py
@@ -59,12 +59,6 @@
     gate_ref,
     out_ref,
     tokens,
-    wq_ret,
-    wk_ret,
-    wv_ret,
-    wq_att,
-    wk_att,
-    wv_att,
     table,
     xbuf,
     abuf,
@@ -93,13 +87,13 @@
     loads = [
         pltpu.make_async_copy(source, target, load.at[k])
         for k, (source, target) in enumerate((
-            (wk_att_hbm, wk_att),
-            (wv_att_hbm, wv_att),
-            (wk_ret_hbm, wk_ret),
-            (wv_ret_hbm, wv_ret),
+            (wk_att_hbm, abuf.at[me, pl.ds(0, HEAD)]),
+            (wv_att_hbm, abuf.at[me, pl.ds(HEAD, HEAD)]),
+            (wk_ret_hbm, abuf.at[me, pl.ds(2 * HEAD, width)]),
+            (wv_ret_hbm, abuf.at[me, pl.ds(2 * HEAD + width, width)]),
             (tok_hbm, tokens),
-            (wq_att_hbm, wq_att),
-            (wq_ret_hbm, wq_ret),
+            (wq_att_hbm, bbuf.at[me, pl.ds(0, width)]),
+            (wq_ret_hbm, bbuf.at[me, pl.ds(width, width)]),
             (table_hbm.at[pl.ds(pl.multiple_of(me * tok, tok), tok)], table),
             (wo_ret_hbm, obuf.at[me, pl.ds(0, half_o)]),
             (wo_att_hbm, obuf.at[me, pl.ds(half_o, wo_att_hbm.shape[0])]),
@@ -116,10 +110,6 @@
 
     for copy in loads[:4]:
         copy.wait()
-    abuf[me, :, :HEAD] = wk_att[...]
-    abuf[me, :, HEAD : 2 * HEAD] = wv_att[...]
-    abuf[me, :, 2 * HEAD : 2 * HEAD + width] = wk_ret[...]
-    abuf[me, :, 2 * HEAD + width :] = wv_ret[...]
     pl.semaphore_wait(barrier, 2 + m - 1)
 
     def ring_copy(buf, send, recv, pieces, step, way, chunk, arriving):
@@ -174,8 +164,6 @@
     ring_step(ring_a, 1)
     for copy in loads[5:]:
         copy.wait()
-    bbuf[me, :, :width] = wq_att[...]
-    bbuf[me, :, width:] = wq_ret[...]
     ring_step(ring_a, 2)
 
     lines = lax.broadcasted_iota(jnp.int32, (tok, tok), 0)
@@ -218,7 +206,13 @@
             [first * cosine - second * sine, first * sine + second * cosine], axis=-1
         )
 
-    proj = dot(xbuf[...], abuf[...].reshape(-1, abuf.shape[2]))
+    def project(buf):
+        deep = buf.shape[2]
+        return sum(
+            dot(xbuf[:, k * deep : (k + 1) * deep], buf[k], ((1,), (1,))) for k in range(n)
+        )
+
+    proj = project(abuf)
     pair = proj[:, : 2 * HEAD].astype(BF16)
     keys, vals, updates, marks = [], [], [], []
     for h in range(heads):
@@ -255,7 +249,7 @@
         if step + 2 <= n - 1:
             ring_step(ring_b, step + 2)
 
-    projq = dot(xbuf[...], bbuf[...].reshape(-1, bbuf.shape[2]))
+    projq = project(bbuf)
     ring_step(ring_o, 1)
     local, lifts = [], []
     for h in range(heads):
@@ -396,16 +390,10 @@
         out_specs=vmem,
         scratch_shapes=[
             pltpu.VMEM(tokens.shape, BF16),
-            pltpu.VMEM(w_query_ret.shape, BF16),
-            pltpu.VMEM(w_key_ret.shape, BF16),
-            pltpu.VMEM(w_value_ret.shape, BF16),
-            pltpu.VMEM(w_query_att.shape, BF16),
-            pltpu.VMEM(w_key_att.shape, BF16),
-            pltpu.VMEM(w_value_att.shape, BF16),
             pltpu.VMEM((tok, HEAD), F32),
             pltpu.VMEM((tok, depth), BF16),
-            pltpu.VMEM((n, deep, wide_a), BF16),
-            pltpu.VMEM((n, deep, wide_b), BF16),
+            pltpu.VMEM((n, wide_a, deep), BF16),
+            pltpu.VMEM((n, wide_b, deep), BF16),
             pltpu.VMEM((n, deep_o, w_out_ret.shape[1]), BF16),
             pltpu.VMEM((n, tall, 2 * HEAD), BF16),
             pltpu.VMEM((heads, HEAD, HEAD), F32),
@@ -426,12 +414,12 @@
     )(
         tokens,
         pre_gain[None, :],
-        w_query_ret,
-        w_key_ret,
-        w_value_ret,
-        w_query_att,
-        w_key_att,
-        w_value_att,
+        w_query_ret.T,
+        w_key_ret.T,
+        w_value_ret.T,
+        w_query_att.T,
+        w_key_att.T,
+        w_value_att.T,
         w_out_ret,
         w_out_att,
         jnp.asarray(table),

time: 95.7 us -> 89.8 us (0.938)
  local copies, waits for them, and re-layouts: 7.36 us -> 1.67 us
    unnamed x17 -> x1, local copies, waits for them, and re-layouts: 7.36 us -> 1.67 us
where the time goes in v3:
time: 89.8 us; the launch traced here: 89.6 us
  Pallas kernels  87.9 us (98%)
  local copies, waits for them, and re-layouts  1.67 us (2%)
    pallas_call x1, Pallas kernels, body(): pl.pallas_call(functools.partial(kernel, n, m, heads, chunks), out_shape=...  87.9 us

profile of v3, /device:TPU:1, one launch (start us, length us, event | category | flops | bytes accessed | tf_op | source)
XLA Modules:
  0.0 89.6 jit_solution(16839806593473751464)
XLA Ops:
  0.0 87.9 %shard_map.127 = bf16[64,2048]{1,0:T(8,128)(2,1)} custom-call(bf16[64,2048]{1,0:T(8,128)(2,1)} %tok_hbm.1, f32[1,2048]{1,0:T(1,128)} %bitcast.14, bf16[192,256]{1,0:T(8,128)(2,1)} %bitcast.8, bf16[192,256]{1,0:T(8,128)(2,1)} %bitcast.9, bf16[192,256]{1,0:T(8,128)(2,1)} %bitcast.10, bf16[192,256]{1,0:T(8,128)(2,1)} %bitcast.11, bf16[64,256]{1,0:T(8,128)(2,1)} %bitcast.12, ...), custom_call_target="tpu_custom_call" | custom-call | tf_op jit(solution)/shard_map/pallas_call | solution.py:386
  87.9 1.7 %copy.15 = bf16[64,2048]{1,0:T(8,128)(2,1)} copy(bf16[64,2048]{1,0:T(8,128)(2,1)} %shard_map.127) | data formatting | bytes 524288

commit v4 on v3

--- a/solution.py
+++ b/solution.py
@@ -112,12 +112,14 @@
         copy.wait()
     pl.semaphore_wait(barrier, 2 + m - 1)
 
+    rounds = n // 2
+    full = (n - 1) // 2
+
     def ring_copy(buf, send, recv, pieces, step, way, chunk, arriving):
         hops = step + 1 if arriving else step
         owner = ring_to_sp((place + (n - hops if way == 0 else hops)) % n, n)
-        half = buf.shape[1] // 2
-        piece = half // pieces
-        span = pl.ds(way * half + chunk * piece, piece)
+        piece = buf.shape[1] // pieces
+        span = pl.ds(chunk * piece, piece)
         return pltpu.make_async_remote_copy(
             src_ref=buf.at[owner, span],
             dst_ref=buf.at[owner, span],
@@ -129,12 +131,17 @@
 
     started = []
 
+    def travels(pieces, step, way, chunk):
+        if step < full:
+            return True
+        return step < rounds and (chunk < pieces // 2) == (way == 0)
+
     def ring_step(group, step):
         for chunk in range(group[3]):
             for way in range(2):
-                if step > 0:
+                if step > 0 and travels(group[3], step - 1, way, chunk):
                     ring_copy(*group, step - 1, way, chunk, True).wait_recv()
-                if step < n - 1:
+                if travels(group[3], step, way, chunk):
                     copy = ring_copy(*group, step, way, chunk, False)
                     copy.start()
                     started.append(copy)
@@ -161,11 +168,8 @@
         )
         copy.start()
         started.append(copy)
-    ring_step(ring_a, 1)
     for copy in loads[5:]:
         copy.wait()
-    ring_step(ring_a, 2)
-
     lines = lax.broadcasted_iota(jnp.int32, (tok, tok), 0)
     across = lax.broadcasted_iota(jnp.int32, (tok, tok), 1)
     causal = lines >= across
@@ -183,7 +187,7 @@
     ).T
     cosine, sine = table[:, : HEAD // 2], table[:, HEAD // 2 :]
 
-    for step in range(3, n - 1):
+    for step in range(1, rounds):
         ring_step(ring_a, step)
     ring_step(ring_b, 0)
     for r in range(1, m):
@@ -196,7 +200,7 @@
             device_id={"tp": (mine + r) % m},
             device_id_type=MESH,
         ).wait_recv()
-    ring_step(ring_a, n - 1)
+    ring_step(ring_a, rounds)
     ring_step(ring_b, 1)
 
     def rope(field):
@@ -242,14 +246,14 @@
         lanes = slice(k % 2 * HEAD, (k % 2 + 1) * HEAD)
         return kvbuf[index, tok + k // 2 * HEAD : tok + (k // 2 + 1) * HEAD, lanes].astype(F32)
 
-    for step in range(n - 1):
+    for step in range(rounds - 1):
         ring_step(ring_k, step)
-        if step == n - 2:
-            ring_step(ring_o, 0)
-        if step + 2 <= n - 1:
-            ring_step(ring_b, step + 2)
+        ring_step(ring_b, step + 2)
+    ring_step(ring_k, rounds - 1)
+    ring_step(ring_o, 0)
 
     projq = project(bbuf)
+    ring_step(ring_k, rounds)
     ring_step(ring_o, 1)
     local, lifts = [], []
     for h in range(heads):
@@ -261,7 +265,6 @@
         weights = jnp.where(causal, scores * jnp.exp(gap), 0.0).astype(BF16)
         local.append(dot(weights, vals[h]))
         lifts.append((query.astype(F32) * jnp.exp(column)).astype(BF16))
-    ring_step(ring_o, 2)
 
     queries = [
         (projq[:, h * HEAD : (h + 1) * HEAD] * HEAD ** (-0.5)).astype(BF16) for h in range(heads)
@@ -284,7 +287,8 @@
     num[...] = jnp.zeros_like(num)
     state[...] = jnp.zeros_like(state)
     attend(me, True)
-    ring_step(ring_k, n - 1)
+    pending = list(range(2, rounds + 1))
+    ring_step(ring_o, pending.pop(0))
     for j in range(n - 1):
         def earlier(j=j):
             marked = piece_of(j, heads)
@@ -294,9 +298,9 @@
             attend(j, False)
 
         pl.when(me > j)(earlier)
-        if 3 + j <= n - 1:
-            ring_step(ring_o, 3 + j)
-    for step in range(3 + n - 1, n):
+        if j % 3 == 2 and len(pending) > 1:
+            ring_step(ring_o, pending.pop(0))
+    for step in pending:
         ring_step(ring_o, step)
 
     retained, attended = [], []
@@ -381,7 +385,7 @@
     hbm = pl.BlockSpec(memory_space=pl.ANY)
     vmem = pl.BlockSpec(memory_space=pltpu.VMEM)
     dma = pltpu.SemaphoreType.DMA
-    rings = [dma((2, n - 1, c)) for c in chunks for _ in range(2)]
+    rings = [dma((2, n // 2, c)) for c in chunks for _ in range(2)]
     parts = n // 2 if n % 2 == 0 else n
     return pl.pallas_call(
         functools.partial(kernel, n, m, heads, chunks),
@@ -618,7 +622,7 @@
     whole_tiles = w_out_ret.shape[1] % LANES == 0 and w_key_ret.shape[0] % LANES == 0
     heads = arrays[10].shape[1]
     small = 16 * heads <= HEAD and arrays[7].shape[1] == HEAD and arrays[11].shape[0] == heads
-    if whole_tiles and small and tokens.shape[0] * m == SPAN:
+    if n % 2 == 0 and n > 2 and whole_tiles and small and tokens.shape[0] * m == SPAN:
         return body(n, m, *arrays)
     return plain_body(*arrays)
 

time: 89.8 us -> 82.8 us (0.922); the launches traced: 89.6 us -> 81.4 us
  Pallas kernels: 87.9 us -> 79.7 us
    pallas_call x1, Pallas kernels: 87.9 us -> 79.7 us  [body(): pl.pallas_call(functools.partial(kernel, n, m, heads, chunks), out_shape=...]
where the time goes in v4:
time: 82.8 us; the launch traced here: 81.4 us
  Pallas kernels  79.7 us (96%)
  local copies, waits for them, and re-layouts  1.67 us (2%)
    pallas_call x1, Pallas kernels, body(): pl.pallas_call(functools.partial(kernel, n, m, heads, chunks), out_shape=...  79.7 us
    unnamed x1, local copies, waits for them, and re-layouts  1.67 us

profile of v4, /device:TPU:1, one launch (start us, length us, event | category | flops | bytes accessed | tf_op | source)
XLA Modules:
  0.0 81.4 jit_solution(15576057462316063861)
XLA Ops:
  0.0 79.7 %shard_map.127 = bf16[64,2048]{1,0:T(8,128)(2,1)} custom-call(bf16[64,2048]{1,0:T(8,128)(2,1)} %tok_hbm.1, f32[1,2048]{1,0:T(1,128)} %bitcast.14, bf16[192,256]{1,0:T(8,128)(2,1)} %bitcast.8, bf16[192,256]{1,0:T(8,128)(2,1)} %bitcast.9, bf16[192,256]{1,0:T(8,128)(2,1)} %bitcast.10, bf16[192,256]{1,0:T(8,128)(2,1)} %bitcast.11, bf16[64,256]{1,0:T(8,128)(2,1)} %bitcast.12, ...), custom_call_target="tpu_custom_call" | custom-call | tf_op jit(solution)/shard_map/pallas_call | solution.py:390
  79.7 1.7 %copy.15 = bf16[64,2048]{1,0:T(8,128)(2,1)} copy(bf16[64,2048]{1,0:T(8,128)(2,1)} %shard_map.127) | data formatting | bytes 524288
